TPU v7x, 32 devices: a whole 2x2x4 slice. The times are simulated.
32 devices in a mesh: fs: 16 (over z, y, x), tp: 2 (over core).
Axes of the slice: x: 2, y: 2, z: 4, core: 2. Of those that a mesh axis runs over, the one named last changes fastest.
Arguments:
- tokens: bfloat16 [12288, 2048], P('fs'), may hold values from -6 to 6
- norm_gain: float32 [2048], replicated, may hold values from 0.1 to 1.9
- up_weight: float32 [2048, 8192], P('fs', 'tp'), may hold values from -0.125 to 0.125
- up_scale: float32 [8192], P('tp'), may hold values from 0.5 to 2
- down_weight: float32 [8192, 2048], P('tp', 'fs'), may hold values from -0.09375 to 0.09375
- down_scale: float32 [1, 2048], replicated, may hold values from 0.5 to 2
Outputs:
- mixed: bfloat16 [12288, 2048], P('fs', 'tp')
All inputs are finite; a program needn't handle non-finite values.
Results may differ from a plain program's by a relative error of at most 0.014.
Values may be sent and summed in bfloat16 or wider, within the bound.
A program may use at most 128 MiB of HBM per device.

v0:
```python
import jax
import jax.numpy as jnp
from jax import lax
from jax.sharding import PartitionSpec as P


def on_device(tokens, norm_gain, up_weight, up_scale, down_weight, down_scale):
    values = tokens.astype(jnp.float32)
    normed = (
        values * lax.rsqrt(jnp.mean(values * values, axis=-1, keepdims=True) + 1e-06) * norm_gain
    ).astype(jnp.bfloat16)
    up_cast = up_weight.astype(jnp.bfloat16)
    down_cast = down_weight.astype(jnp.bfloat16)
    up_full = lax.all_gather(up_cast, "fs", axis=0, tiled=True)
    pre = jnp.dot(normed, up_full, preferred_element_type=jnp.float32) * up_scale
    hidden = jnp.square(jnp.maximum(pre, 0.0)).astype(jnp.bfloat16)
    down_full = lax.all_gather(down_cast, "fs", axis=1, tiled=True)
    partial_value = jnp.dot(hidden, down_full, preferred_element_type=jnp.float32) * down_scale
    rounded = partial_value.astype(jnp.bfloat16)
    return (
        lax.psum_scatter(rounded, "tp", scatter_dimension=1, tiled=True)
        .astype(jnp.float32)
        .astype(jnp.bfloat16)
    )


def solution(mesh):
    in_specs = (P("fs", None), P(), P("fs", "tp"), P("tp"), P("tp", "fs"), P())
    out_specs = P("fs", "tp")
    return jax.shard_map(
        on_device, mesh=mesh, in_specs=in_specs, out_specs=out_specs, check_vma=False
    )
```

profile of v0, /device:TPU:0, one launch (start us, length us, event | category | flops | bytes accessed | tf_op | source)
XLA Modules:
  0.0 508.0 jit_solution(3920290398394496879)
XLA Ops:
  6.5 0.0 copy-start
  6.5 0.0 copy-start.2
  6.5 0.0 copy-start.1
  6.5 0.0 copy-start.3
  6.5 0.0 all-gather.3.cloned.1.call-start
  6.6 2.8 convert_element_type.22
  9.4 0.0 all-gather.3.cloned.1.call-update
  9.5 0.0 all-gather.5.cloned.1.call-start
  9.5 2.7 convert_element_type.24
  12.2 0.0 all-gather.5.cloned.1.call-update
  12.2 0.0 reduce-scatter.2.cloned.1.call-start
  12.2 0.0 copy-done
  12.3 0.7 fusion
  13.0 190.9 %all-gather.3.cloned.1.call-done = bf16[2048,4096]{1,0:T(8,128)(2,1)} async-done(((bf16[128,4096]{1,0:T(8,128)(2,1)}), bf16[2048,4096]{1,0:T(8,128)(2,1)}) %all-gather.3.cloned.1.call-update) | async-done | bytes 16777232 | tf_op jit(solution)/shard_map/all_gather | solution.py:14
  203.9 250.0 %all-gather.5.cloned.1.call-done = bf16[4096,2048]{1,0:T(8,128)(2,1)} async-done(((bf16[4096,128]{1,0:T(8,128)(2,1)}), bf16[4096,2048]{1,0:T(8,128)(2,1)}) %all-gather.5.cloned.1.call-update) | async-done | bytes 16777232 | tf_op jit(solution)/shard_map/all_gather | solution.py:17
  453.9 0.0 copy-done.2
  453.9 0.0 copy-done.1
  453.9 0.0 copy-done.3
  453.9 38.3 %multiply_convert_fusion.1 = bf16[768,2048]{1,0:T(8,128)(2,1)} fusion(bf16[4096,2048]{1,0:T(8,128)(2,1)} %all-gather.5.cloned.1.call-done, f32[2048]{0:T(1024)S(1)} %bitcast.8, bf16[2048,4096]{1,0:T(8,128)(2,1)} %all-gather.3.cloned.1.call-done, f32[4096]{0:T(1024)S(1)} %copy-done.1, bf16[768,2048]{1,0:T(8,128)(2,1)S(1)} %copy-done, f32[2048]{0:T(1024)S(1)} %copy-done.3, ...), kind=kOutput, calls=%fused_computation.6 | convolution fusion | flops 25791823872 | bytes 39881728 | tf_op jit(solution)/shard_map/dot_general | solution.py:18
  492.2 0.0 reduce-scatter.2.cloned.1.call-update
  492.2 9.3 %reduce-scatter.2.cloned.1.call-done = bf16[768,1024]{1,0:T(8,128)(2,1)} async-done(((bf16[768,2048]{1,0:T(8,128)(2,1)}), bf16[768,1024]{1,0:T(8,128)(2,1)}) %reduce-scatter.2.cloned.1.call-update) | async-done | bytes 1572880 | tf_op jit(solution)/shard_map/reduce_scatter | solution.py:21
  (1 shorter events, 0.0 us)
Async XLA Ops:
  6.5 5.7 %copy-start = (bf16[768,2048]{1,0:T(8,128)(2,1)S(1)}, bf16[768,2048]{1,0:T(8,128)(2,1)}, u32[]{:S(2)}) copy-start(bf16[768,2048]{1,0:T(8,128)(2,1)} %param.6) | copy-start | bytes 9437188
  6.5 447.4 %copy-start.2 = (f32[1,2048]{1,0:T(1,128)S(1)}, f32[1,2048]{1,0:T(1,128)}, u32[]{:S(2)}) copy-start(f32[1,2048]{1,0:T(1,128)} %param.11) | copy-start | bytes 24580
  6.5 447.4 %copy-start.1 = (f32[4096]{0:T(1024)S(1)}, f32[4096]{0:T(1024)}, u32[]{:S(2)}) copy-start(f32[4096]{0:T(1024)} %param.9) | copy-start | bytes 49156
  6.5 447.4 %copy-start.3 = (f32[2048]{0:T(1024)S(1)}, f32[2048]{0:T(1024)}, u32[]{:S(2)}) copy-start(f32[2048]{0:T(1024)} %param.7) | copy-start | bytes 24580
  6.5 197.3 %all-gather.3.cloned.1.call-start = ((), (), s32[]{:S(2)}) async-start(), calls=%async_computation.1 | async-start | bytes 17825792 | tf_op jit(solution)/shard_map/all_gather | solution.py:14
  9.5 444.4 %all-gather.5.cloned.1.call-start = ((), (), s32[]{:S(2)}) async-start(), calls=%async_computation.2 | async-start | bytes 17825792 | tf_op jit(solution)/shard_map/all_gather | solution.py:17
  12.2 489.3 %reduce-scatter.2.cloned.1.call-start = ((), (), s32[]{:S(2)}) async-start(), calls=%async_computation.3 | async-start | bytes 4718592 | tf_op jit(solution)/shard_map/reduce_scatter | solution.py:21
Sparse Core Ops, SparseCore 0:
  10.1 193.7 all-gather.2
  206.6 247.2 all-gather.4
  492.3 9.1 reduce-scatter.1
where the time goes:
time: 508 us
  waiting for transfers between devices  450 us (89%)
  matrix products  38.3 us (8%)
  between operations  13.1 us (3%)
  other arithmetic  6.2 us (1%)
    all_gather x1, waiting for transfers between devices, on_device(): down_full = lax.all_gather(down_cast, 'fs', axis=1, tiled=True)  250 us
    all_gather x1, waiting for transfers between devices, on_device(): up_full = lax.all_gather(up_cast, 'fs', axis=0, tiled=True)  191 us
    dot_general x1, matrix products, on_device(): jnp.dot(hidden, down_full, preferred_element_type=jnp.float32) * down_scale  38.3 us
  transfers between devices with their start and end apart: 3, of which 3 were waited for; matrix products, arithmetic and copies ran while one was open for 1% of the time, Pallas kernels for 0%

commit v1 on v0

--- a/solution.py
+++ b/solution.py
@@ -14,7 +14,7 @@
     up_full = lax.all_gather(up_cast, "fs", axis=0, tiled=True)
     pre = jnp.dot(normed, up_full, preferred_element_type=jnp.float32) * up_scale
     hidden = jnp.square(jnp.maximum(pre, 0.0)).astype(jnp.bfloat16)
-    down_full = lax.all_gather(down_cast, "fs", axis=1, tiled=True)
+    down_full = jnp.concatenate(lax.all_gather(down_cast, axis_name="fs"), 1)
     partial_value = jnp.dot(hidden, down_full, preferred_element_type=jnp.float32) * down_scale
     rounded = partial_value.astype(jnp.bfloat16)
     return (

time: 508 us -> 451 us (0.89)
  waiting for transfers between devices: 450 us -> 371 us
  local copies, waits for them, and re-layouts: 0.01 us -> 21 us
    all_gather x1, waiting for transfers between devices: 250 us -> 191 us  [on_device(): down_full = jnp.concatenate(lax.all_gather(down_cast, axis_name='fs'), 1)]
    reshape x0 -> x1, local copies, waits for them, and re-layouts: none -> 21 us  [on_device(): down_full = jnp.concatenate(lax.all_gather(down_cast, axis_name='fs'), 1)]
    all_gather x1, waiting for transfers between devices: 191 us -> 171 us  [on_device(): up_full = lax.all_gather(up_cast, 'fs', axis=0, tiled=True)]
    dot_general x1, matrix products: 38.3 us -> 19.8 us  [on_device(): jnp.dot(hidden, down_full, preferred_element_type=jnp.float32) * down_scale]
    dot_general x0 -> x1, matrix products: none -> 18.5 us  [on_device(): jnp.dot(normed, up_full, preferred_element_type=jnp.float32) * up_scale]
  transfers between devices with their start and end apart: 3 -> 3, of which waited for: 3 -> 3; matrix products, arithmetic and copies ran while one was open for 1% -> 5% of each run, Pallas kernels for 0% -> 0%
where the time goes in v1:
time: 451 us; the launch traced here: 450 us
  waiting for transfers between devices  371 us (82%)
  matrix products  38.2 us (8%)
  local copies, waits for them, and re-layouts  21 us (5%)
  between operations  13.1 us (3%)
  other arithmetic  6.2 us (1%)
    all_gather x1, waiting for transfers between devices, on_device(): down_full = jnp.concatenate(lax.all_gather(down_cast, axis_name='fs'), 1)  191 us
    all_gather x1, waiting for transfers between devices, on_device(): up_full = lax.all_gather(up_cast, 'fs', axis=0, tiled=True)  171 us
    reshape x1, local copies, waits for them, and re-layouts, on_device(): down_full = jnp.concatenate(lax.all_gather(down_cast, axis_name='fs'), 1)  21 us
    dot_general x1, matrix products, on_device(): jnp.dot(hidden, down_full, preferred_element_type=jnp.float32) * down_scale  19.8 us
    dot_general x1, matrix products, on_device(): jnp.dot(normed, up_full, preferred_element_type=jnp.float32) * up_scale  18.5 us
    reduce_scatter x1, waiting for transfers between devices, on_device(): lax.psum_scatter(rounded, 'tp', scatter_dimension=1, tiled=True)  9.32 us
  transfers between devices with their start and end apart: 3, of which 3 were waited for; matrix products, arithmetic and copies ran while one was open for 5% of the time, Pallas kernels for 0%

profile of v1, /device:TPU:0, one launch (start us, length us, event | category | flops | bytes accessed | tf_op | source)
XLA Modules:
  0.0 449.9 jit_solution(5662449550664147701)
XLA Ops:
  6.5 0.0 copy-start
  6.5 0.0 all-gather.6.cloned.1.call-start
  6.5 2.8 convert_element_type.24
  9.4 0.0 all-gather.6.cloned.1.call-update
  9.4 0.0 all-gather.4.cloned.1.call-start
  9.4 2.7 convert_element_type.22
  12.1 0.0 all-gather.4.cloned.1.call-update
  12.1 0.0 reduce-scatter.2.cloned.1.call-start
  12.2 0.0 copy-done
  12.2 0.7 fusion
  12.9 191.0 %all-gather.6.cloned.1.call-done = bf16[65536,128]{1,0:T(8,128)(2,1)} async-done(((bf16[4096,128]{1,0:T(8,128)(2,1)}), bf16[65536,128]{1,0:T(8,128)(2,1)}) %all-gather.6.cloned.1.call-update) | async-done | bytes 16777232 | tf_op jit(solution)/shard_map/all_gather | solution.py:17
  203.9 0.0 copy-start.1
  203.9 0.0 copy-start.2
  203.9 21.0 %copy.7 = bf16[4096,16,128]{0,2,1:T(8,128)(2,1)} copy(bf16[4096,16,128]{2,0,1:T(8,128)(2,1)} %bitcast.20) | data formatting | bytes 33554432 | tf_op jit(solution)/shard_map/reshape | solution.py:17
  224.9 0.0 copy-start.3
  224.9 171.0 %all-gather.4.cloned.1.call-done = bf16[2048,4096]{1,0:T(8,128)(2,1)} async-done(((bf16[128,4096]{1,0:T(8,128)(2,1)}), bf16[2048,4096]{1,0:T(8,128)(2,1)}) %all-gather.4.cloned.1.call-update) | async-done | bytes 16777232 | tf_op jit(solution)/shard_map/all_gather | solution.py:14
  395.8 0.0 copy-done.1
  395.8 0.0 copy-done.2
  395.8 18.5 %fusion.26 = bf16[768,4096]{1,0:T(8,128)(2,1)} fusion(f32[4096]{0:T(1024)S(1)} %copy-done.1, bf16[2048,4096]{1,0:T(8,128)(2,1)} %all-gather.4.cloned.1.call-done, bf16[768,2048]{1,0:T(8,128)(2,1)S(1)} %copy-done, f32[2048]{0:T(1024)S(1)} %copy-done.2, f32[768]{0:T(1024)S(1)} %add_rsqrt_fusion), kind=kOutput, calls=%bitcast_fusion.clone.1 | convolution fusion | flops 12903776256 | bytes 26242048 | tf_op jit(solution)/shard_map/dot_general | solution.py:15
  414.3 0.0 copy-done.3
  414.3 19.8 %multiply_convert_fusion.1 = bf16[768,2048]{1,0:T(8,128)(2,1)} fusion(bf16[4096,2048]{0,1:T(8,128)(2,1)} %bitcast.21, f32[2048]{0:T(1024)S(1)} %bitcast.22, bf16[768,4096]{1,0:T(8,128)(2,1)} %fusion.26), kind=kOutput, calls=%fused_computation.6 | convolution fusion | flops 12888047616 | bytes 26222592 | tf_op jit(solution)/shard_map/dot_general | solution.py:18
  434.1 0.0 reduce-scatter.2.cloned.1.call-update
  434.1 9.3 %reduce-scatter.2.cloned.1.call-done = bf16[768,1024]{1,0:T(8,128)(2,1)} async-done(((bf16[768,2048]{1,0:T(8,128)(2,1)}), bf16[768,1024]{1,0:T(8,128)(2,1)}) %reduce-scatter.2.cloned.1.call-update) | async-done | bytes 1572880 | tf_op jit(solution)/shard_map/reduce_scatter | solution.py:21
  (1 shorter events, 0.0 us)
Async XLA Ops:
  6.5 5.7 %copy-start = (bf16[768,2048]{1,0:T(8,128)(2,1)S(1)}, bf16[768,2048]{1,0:T(8,128)(2,1)}, u32[]{:S(2)}) copy-start(bf16[768,2048]{1,0:T(8,128)(2,1)} %param.6) | copy-start | bytes 9437188
  6.5 197.3 %all-gather.6.cloned.1.call-start = ((), (), s32[]{:S(2)}) async-start(), calls=%async_computation.3 | async-start | bytes 17825792 | tf_op jit(solution)/shard_map/all_gather | solution.py:17
  9.4 386.5 %all-gather.4.cloned.1.call-start = ((), (), s32[]{:S(2)}) async-start(), calls=%async_computation.1 | async-start | bytes 17825792 | tf_op jit(solution)/shard_map/all_gather | solution.py:14
  12.1 431.3 %reduce-scatter.2.cloned.1.call-start = ((), (), s32[]{:S(2)}) async-start(), calls=%async_computation.2 | async-start | bytes 4718592 | tf_op jit(solution)/shard_map/reduce_scatter | solution.py:21
  203.9 192.0 %copy-start.1 = (f32[4096]{0:T(1024)S(1)}, f32[4096]{0:T(1024)}, u32[]{:S(2)}) copy-start(f32[4096]{0:T(1024)} %param.9) | copy-start | bytes 49156
  203.9 192.0 %copy-start.2 = (f32[2048]{0:T(1024)S(1)}, f32[2048]{0:T(1024)}, u32[]{:S(2)}) copy-start(f32[2048]{0:T(1024)} %param.7) | copy-start | bytes 24580
  224.9 189.4 %copy-start.3 = (f32[1,2048]{1,0:T(1,128)S(1)}, f32[1,2048]{1,0:T(1,128)}, u32[]{:S(2)}) copy-start(f32[1,2048]{1,0:T(1,128)} %param.11) | copy-start | bytes 24580
Sparse Core Ops, SparseCore 0:
  10.1 193.7 all-gather.5
  206.6 189.1 all-gather.3
  434.2 9.1 reduce-scatter.1
